TPU v7x, 128 devices: a whole 4x4x4 slice. The times are simulated.
128 devices in a mesh: fs: 16 (over z, y), tp: 8 (over x, core).
Axes of the slice: x: 4, y: 4, z: 4, core: 2. Of those that a mesh axis runs over, the one named last changes fastest.
Arguments:
- tokens: bfloat16 [16384, 2048], P(('fs', 'tp')), may hold values from -6 to 6
- norm_gain: float32 [2048], replicated, may hold values from 0.1 to 1.9
- up_weight: float32 [2048, 8192], P('fs', 'tp'), may hold values from -0.125 to 0.125
- down_weight: float32 [8192, 2048], P('tp', 'fs'), may hold values from -0.0625 to 0.0625
Outputs:
- mlp_out: bfloat16 [16384, 2048], P(('fs', 'tp'))
All inputs are finite; a program needn't handle non-finite values.
Results may differ from a plain program's by a relative error of at most 0.0017.
Values may be sent and summed in bfloat16 or wider, within the bound.
A program may use at most 64 MiB of HBM per device.

v0:
```python
import jax
import jax.numpy as jnp
from jax import lax
from jax.sharding import PartitionSpec as P

epsilon = 1e-06


def taken_in(slab, axis, dim, step, start):

    def gathered(part):
        return lax.all_gather(part, axis, axis=dim, tiled=True)

    return step(start, jax.tree.map(gathered, slab), jnp.int32(0))


def on_whole(shard, axis, dim, work):
    return work(lax.all_gather(shard, axis, axis=dim, tiled=True), jnp.int32(0))


def shards(tokens, norm_gain, up_weight, down_weight):
    values = tokens.astype(jnp.float32)
    scale = lax.rsqrt(jnp.mean(values * values, axis=-1, keepdims=True) + epsilon)
    normed = (values * scale * norm_gain).astype(jnp.bfloat16)
    grouped = lax.all_gather(normed, "tp", axis=0, tiled=True)
    empty = jnp.zeros((grouped.shape[0], up_weight.shape[1]), jnp.float32)

    def add_rows(total, piece, start):
        columns = lax.dynamic_slice_in_dim(grouped, start, piece.shape[0], 1)
        return total + jnp.dot(
            columns, piece.astype(jnp.bfloat16), preferred_element_type=jnp.float32
        )

    pre = taken_in(up_weight.astype(jnp.bfloat16), "fs", 0, add_rows, empty)
    hidden = jnp.square(jax.nn.relu(pre)).astype(jnp.bfloat16)

    def project(piece, start):
        return jnp.dot(hidden, piece.astype(jnp.bfloat16), preferred_element_type=jnp.float32)

    terms = on_whole(down_weight.astype(jnp.bfloat16), "fs", 1, project)
    summed = lax.psum_scatter(terms, "tp", scatter_dimension=0, tiled=True)
    return summed.astype(jnp.bfloat16)


def solution(mesh):
    placed = (P(("fs", "tp"), None), P(), P("fs", "tp"), P("tp", "fs"))
    return jax.shard_map(
        shards, mesh=mesh, in_specs=placed, out_specs=P(("fs", "tp"), None), check_vma=False
    )
```

profile of v0, /device:TPU:1, one launch (start us, length us, event | category | flops | bytes accessed | tf_op | source)
XLA Modules:
  0.0 232.5 jit_solution(14041995372060814346)
XLA Ops:
  6.5 0.0 all-gather.4.cloned.1.call-start
  6.5 1.2 fusion
  7.8 2.0 fusion.2
  9.8 0.0 all-gather.4.cloned.1.call-update
  9.8 0.0 all-gather.6.cloned.1.call-start
  9.9 1.8 convert_element_type.20
  11.7 0.0 all-gather.6.cloned.1.call-update
  11.7 0.0 all-gather.8.cloned.1.call-start
  11.7 1.8 convert_element_type.22
  13.5 0.0 all-gather.8.cloned.1.call-update
  13.5 0.0 reduce-scatter.2.cloned.1.call-start
  13.6 32.0 %all-gather.4.cloned.1.call-done = bf16[1024,2048]{1,0:T(8,128)(2,1)} async-done(((bf16[128,2048]{1,0:T(8,128)(2,1)}), bf16[1024,2048]{1,0:T(8,128)(2,1)}) %all-gather.4.cloned.1.call-update) | async-done | bytes 4194320 | tf_op jit(solution)/shard_map/all_gather | solution.py:25
  45.6 53.1 %all-gather.6.cloned.1.call-done = bf16[2048,1024]{1,0:T(8,128)(2,1)} async-done(((bf16[128,1024]{1,0:T(8,128)(2,1)}), bf16[2048,1024]{1,0:T(8,128)(2,1)}) %all-gather.6.cloned.1.call-update) | async-done | bytes 4194320 | tf_op jit(solution)/shard_map/all_gather | solution.py:12
  98.7 57.5 %all-gather.8.cloned.1.call-done = bf16[1024,2048]{1,0:T(8,128)(2,1)} async-done(((bf16[1024,128]{1,0:T(8,128)(2,1)}), bf16[1024,2048]{1,0:T(8,128)(2,1)}) %all-gather.8.cloned.1.call-update) | async-done | bytes 4194320 | tf_op jit(solution)/shard_map/all_gather | solution.py:18
  156.2 15.0 %fusion.3 = f32[1024,2048]{1,0:T(8,128)} fusion(bf16[1024,2048]{1,0:T(8,128)(2,1)} %all-gather.8.cloned.1.call-done, bf16[1024,2048]{1,0:T(8,128)(2,1)} %all-gather.4.cloned.1.call-done, bf16[2048,1024]{1,0:T(8,128)(2,1)} %all-gather.6.cloned.1.call-done), kind=kOutput, calls=%fused_computation.6 | convolution fusion | flops 8593080320 | bytes 20971520 | tf_op jit(solution)/shard_map/dot_general | solution.py:38
  171.2 0.0 reduce-scatter.2.cloned.1.call-update
  171.2 52.6 %reduce-scatter.2.cloned.1.call-done = f32[128,2048]{1,0:T(8,128)} async-done(((f32[1024,2048]{1,0:T(8,128)}), f32[128,2048]{1,0:T(8,128)}) %reduce-scatter.2.cloned.1.call-update) | async-done | bytes 1048592 | tf_op jit(solution)/shard_map/reduce_scatter | solution.py:41
  223.9 2.1 convert_element_type.23
  (1 shorter events, 0.0 us)
Async XLA Ops:
  6.5 39.1 %all-gather.4.cloned.1.call-start = ((), (), s32[]{:S(2)}) async-start(), calls=%async_computation.1 | async-start | bytes 4718592 | tf_op jit(solution)/shard_map/all_gather | solution.py:25
  9.8 88.9 %all-gather.6.cloned.1.call-start = ((), (), s32[]{:S(2)}) async-start(), calls=%async_computation.2 | async-start | bytes 4456448 | tf_op jit(solution)/shard_map/all_gather | solution.py:12
  11.7 144.5 %all-gather.8.cloned.1.call-start = ((), (), s32[]{:S(2)}) async-start(), calls=%async_computation.3 | async-start | bytes 4456448 | tf_op jit(solution)/shard_map/all_gather | solution.py:18
  13.5 210.4 %reduce-scatter.2.cloned.1.call-start = ((), (), s32[]{:S(2)}) async-start(), calls=%async_computation.4 | async-start | bytes 9437184 | tf_op jit(solution)/shard_map/reduce_scatter | solution.py:41
Sparse Core Ops, SparseCore 0:
  9.9 35.6 all-gather.3
  47.7 50.9 all-gather.5
  100.8 55.3 all-gather.7
  171.4 52.4 reduce-scatter.1
where the time goes:
time: 233 us
  waiting for transfers between devices  195 us (84%)
  matrix products  15 us (6%)
  between operations  13.1 us (6%)
  other arithmetic  8.9 us (4%)
    all_gather x1, waiting for transfers between devices, on_whole(): return work(lax.all_gather(shard, axis, axis=dim, tiled=True), jnp.int32(0))  57.5 us
    all_gather x1, waiting for transfers between devices, gathered(): return lax.all_gather(part, axis, axis=dim, tiled=True)  53.1 us
    reduce_scatter x1, waiting for transfers between devices, shards(): summed = lax.psum_scatter(terms, 'tp', scatter_dimension=0, tiled=True)  52.6 us
    all_gather x1, waiting for transfers between devices, shards(): grouped = lax.all_gather(normed, 'tp', axis=0, tiled=True)  32 us
    dot_general x1, matrix products, project(): jnp.dot(hidden, piece.astype(jnp.bfloat16), preferred_element_type=jnp.fl...  15 us
  transfers between devices with their start and end apart: 4, of which 4 were waited for; matrix products, arithmetic and copies ran while one was open for 2% of the time, Pallas kernels for 0%

commit v1 on v0

--- a/solution.py
+++ b/solution.py
@@ -4,6 +4,25 @@
 from jax.sharding import PartitionSpec as P
 
 epsilon = 1e-06
+
+
+def follow_the_copies(u):
+    block_now, passed, even = (lax.axis_size("tp"), lax.axis_index("tp"), u.shape[0])
+    current_arr, right_arr = (u, 1)
+    while right_arr < block_now:
+        current_arr = jnp.concatenate(
+            [
+                current_arr,
+                lax.ppermute(
+                    current_arr,
+                    "tp",
+                    [(ix, (ix - right_arr) % block_now) for ix in range(block_now)],
+                ),
+            ],
+            axis=0,
+        )
+        right_arr = 2 * right_arr
+    return jnp.roll(current_arr, passed * even, 0)
 
 
 def taken_in(slab, axis, dim, step, start):
@@ -22,7 +41,7 @@
     values = tokens.astype(jnp.float32)
     scale = lax.rsqrt(jnp.mean(values * values, axis=-1, keepdims=True) + epsilon)
     normed = (values * scale * norm_gain).astype(jnp.bfloat16)
-    grouped = lax.all_gather(normed, "tp", axis=0, tiled=True)
+    grouped = follow_the_copies(normed)
     empty = jnp.zeros((grouped.shape[0], up_weight.shape[1]), jnp.float32)
 
     def add_rows(total, piece, start):

time: 233 us -> 198 us (0.85)
  waiting for transfers between devices: 195 us -> 143 us
  local copies, waits for them, and re-layouts: 0 us -> 8.68 us
  starting transfers between devices: 0.13 us -> 7.5 us
    ppermute x0 -> x3, waiting for transfers between devices: none -> 72.2 us  [follow_the_copies(): lax.ppermute(current_arr, 'tp', [(ix, (ix - right_arr) % block_now) for i...]
    all_gather x1, waiting for transfers between devices: 53.1 us -> 0.01 us  [gathered(): return lax.all_gather(part, axis, axis=dim, tiled=True)]
    all_gather x1, waiting for transfers between devices: 57.5 us -> 18.1 us  [on_whole(): return work(lax.all_gather(shard, axis, axis=dim, tiled=True), jnp.int32(0))]
    all_gather x1 -> x0, waiting for transfers between devices: 32 us -> none  [shards(): grouped = lax.all_gather(normed, 'tp', axis=0, tiled=True)]
    ppermute x0 -> x3, starting transfers between devices: none -> 7.42 us  [follow_the_copies(): lax.ppermute(current_arr, 'tp', [(ix, (ix - right_arr) % block_now) for i...]
    unnamed x0 -> x14, local copies, waits for them, and re-layouts: none -> 7.25 us
  transfers between devices with their start and end apart: 4 -> 6, of which waited for: 4 -> 5; matrix products, arithmetic and copies ran while one was open for 2% -> 8% of each run, Pallas kernels for 0% -> 0%
where the time goes in v1:
time: 198 us
  waiting for transfers between devices  143 us (72%)
  matrix products  15 us (8%)
  between operations  13.1 us (7%)
  other arithmetic  10.5 us (5%)
  local copies, waits for them, and re-layouts  8.68 us (4%)
  starting transfers between devices  7.5 us (4%)
    ppermute x3, waiting for transfers between devices, follow_the_copies(): lax.ppermute(current_arr, 'tp', [(ix, (ix - right_arr) % block_now) for i...  72.2 us
    reduce_scatter x1, waiting for transfers between devices, shards(): summed = lax.psum_scatter(terms, 'tp', scatter_dimension=0, tiled=True)  52.6 us
    all_gather x1, waiting for transfers between devices, on_whole(): return work(lax.all_gather(shard, axis, axis=dim, tiled=True), jnp.int32(0))  18.1 us
    dot_general x1, matrix products, project(): jnp.dot(hidden, piece.astype(jnp.bfloat16), preferred_element_type=jnp.fl...  15 us
    ppermute x3, starting transfers between devices, follow_the_copies(): lax.ppermute(current_arr, 'tp', [(ix, (ix - right_arr) % block_now) for i...  7.42 us
    unnamed x14, local copies, waits for them, and re-layouts  7.25 us
  transfers between devices with their start and end apart: 6, of which 5 were waited for; matrix products, arithmetic and copies ran while one was open for 8% of the time, Pallas kernels for 0%

profile of v1, /device:TPU:1, one launch (start us, length us, event | category | flops | bytes accessed | tf_op | source)
XLA Modules:
  0.0 197.9 jit_solution(9362928776961155883)
XLA Ops:
  6.5 1.8 convert_element_type.20
  8.3 0.0 all-gather.5.cloned.1.call-start
  8.4 1.8 convert_element_type.22
  10.3 1.2 fusion.8
  11.5 2.1 %constant_dynamic-update-slice_fusion.7 = (bf16[2048,2048]{1,0:T(8,128)(2,1)}, bf16[128,2048]{1,0:T(8,128)(2,1)S(1)}) fusion(f32[2048]{0:T(1024)} %param.5, f32[128]{0:T(128)S(1)} %add_rsqrt_fusion, bf16[128,2048]{1,0:T(8,128)(2,1)} %param.4), kind=kLoop, calls=%fused_computation.19 | loop fusion | flops 1048575 | bytes 1581568
  13.6 1.4 collective-permute-start
  15.0 8.1 %collective-permute-done = bf16[128,2048]{1,0:T(8,128)(2,1)S(1)} collective-permute-done((bf16[128,2048]{1,0:T(8,128)(2,1)S(1)}, bf16[128,2048]{1,0:T(8,128)(2,1)S(1)}, u32[]{:S(2)}, u32[]{:S(2)}) %collective-permute-start) | collective-permute-done | bytes 524320 | tf_op jit(solution)/shard_map/ppermute | solution.py:16
  23.0 0.1 pad_maximum_fusion.1
  23.1 3.7 %collective-permute-start.1 = (bf16[256,2048]{1,0:T(8,128)(2,1)S(1)}, bf16[256,2048]{1,0:T(8,128)(2,1)S(1)}, u32[]{:S(2)}, u32[]{:S(2)}) collective-permute-start(bf16[256,2048]{1,0:T(8,128)(2,1)S(1)} %pad_maximum_fusion.1), channel_id=1, source_target_pairs={{0,6},{1,7},{2,0},{3,1},{4,2},{5,3},{6,4},{7,5},{8,14},{9,15},{10,... | collective-permute-start | bytes 3145736 | tf_op jit(solution)/shard_map/ppermute | solution.py:16
  26.8 21.3 %collective-permute-done.1 = bf16[256,2048]{1,0:T(8,128)(2,1)S(1)} collective-permute-done((bf16[256,2048]{1,0:T(8,128)(2,1)S(1)}, bf16[256,2048]{1,0:T(8,128)(2,1)S(1)}, u32[]{:S(2)}, u32[]{:S(2)}) %collective-permute-start.1) | collective-permute-done | bytes 1048608 | tf_op jit(solution)/shard_map/ppermute | solution.py:16
  48.1 1.5 pad_maximum_fusion
  49.6 2.3 %collective-permute-start.2 = (bf16[512,2048]{1,0:T(8,128)(2,1)}, bf16[512,2048]{1,0:T(8,128)(2,1)S(1)}, u32[]{:S(2)}, u32[]{:S(2)}) collective-permute-start(bf16[512,2048]{1,0:T(8,128)(2,1)} %pad_maximum_fusion), channel_id=1, source_target_pairs={{0,4},{1,5},{2,6},{3,7},{4,0},{5,1},{6,2},{7,3},{8,12},{9,13},{10,... | collective-permute-start | bytes 6291464 | tf_op jit(solution)/shard_map/ppermute | solution.py:16
  51.9 2.0 %constant_dynamic-update-slice_fusion.6 = bf16[2048,2048]{1,0:T(8,128)(2,1)} fusion(bf16[2048,2048]{1,0:T(8,128)(2,1)} %get-tuple-element.5, bf16[128,2048]{1,0:T(8,128)(2,1)} %copy-done.2), kind=kLoop, calls=%fused_computation.18 | loop fusion | bytes 1048576
  53.9 1.0 constant_dynamic-update-slice_fusion.5
  54.9 42.9 %collective-permute-done.2 = bf16[512,2048]{1,0:T(8,128)(2,1)S(1)} collective-permute-done((bf16[512,2048]{1,0:T(8,128)(2,1)}, bf16[512,2048]{1,0:T(8,128)(2,1)S(1)}, u32[]{:S(2)}, u32[]{:S(2)}) %collective-permute-start.2) | collective-permute-done | bytes 2097184 | tf_op jit(solution)/shard_map/ppermute | solution.py:16
  97.9 1.5 constant_dynamic-update-slice_fusion.4
  99.3 0.8 constant_dynamic-update-slice_fusion.3
  100.2 0.8 constant_dynamic-update-slice_fusion.2
  101.0 1.0 constant_dynamic-update-slice_fusion.1
  102.1 1.4 constant_dynamic-update-slice_fusion
  103.5 18.1 %all-gather.5.cloned.1.call-done = bf16[1024,2048]{1,0:T(8,128)(2,1)} async-done(((bf16[1024,128]{1,0:T(8,128)(2,1)}), bf16[1024,2048]{1,0:T(8,128)(2,1)}) %all-gather.5.cloned.1.call-update) | async-done | bytes 4194320 | tf_op jit(solution)/shard_map/all_gather | solution.py:37
  121.6 15.0 %fusion.2 = f32[1024,2048]{1,0:T(8,128)} fusion(bf16[1024,2048]{1,0:T(8,128)(2,1)} %all-gather.5.cloned.1.call-done, bf16[2048,1024]{1,0:T(8,128)(2,1)} %all-gather.3.cloned.1.call-done, bf16[2048,2048]{1,0:T(8,128)(2,1)} %constant_dynamic-update-slice_fusion, s32[]{:T(128)S(6)} %select_n.14), kind=kOutput, calls=%fused_computation.3 | convolution fusion | flops 8593080320 | bytes 20971524 | tf_op jit(solution)/shard_map/dot_general | solution.py:57
  136.6 52.6 %reduce-scatter.2.cloned.1.call-done = f32[128,2048]{1,0:T(8,128)} async-done(((f32[1024,2048]{1,0:T(8,128)}), f32[128,2048]{1,0:T(8,128)}) %reduce-scatter.2.cloned.1.call-update) | async-done | bytes 1048592 | tf_op jit(solution)/shard_map/reduce_scatter | solution.py:60
  189.2 2.1 %convert_element_type.23 = bf16[128,2048]{1,0:T(8,128)(2,1)} convert(f32[128,2048]{1,0:T(8,128)} %reduce-scatter.2.cloned.1.call-done) | non-fusion elementwise | flops 262144 | bytes 1572864 | tf_op jit(solution)/shard_map/convert_element_type | solution.py:61
  (15 shorter events, 0.1 us)
Async XLA Ops:
  6.5 97.0 %all-gather.3.cloned.1.call-start = ((), (), s32[]{:S(2)}) async-start(), calls=%async_computation.1 | async-start | bytes 4456448 | tf_op jit(solution)/shard_map/all_gather | solution.py:31
  8.3 113.2 %all-gather.5.cloned.1.call-start = ((), (), s32[]{:S(2)}) async-start(), calls=%async_computation.2 | async-start | bytes 4456448 | tf_op jit(solution)/shard_map/all_gather | solution.py:37
  10.2 179.0 %reduce-scatter.2.cloned.1.call-start = ((), (), s32[]{:S(2)}) async-start(), calls=%async_computation.3 | async-start | bytes 9437184 | tf_op jit(solution)/shard_map/reduce_scatter | solution.py:60
  13.6 34.5 %copy-start = (bf16[128,2048]{1,0:T(8,128)(2,1)}, bf16[128,2048]{1,0:T(8,128)(2,1)S(1)}, u32[]{:S(2)}) copy-start(bf16[128,2048]{1,0:T(8,128)(2,1)S(1)} %get-tuple-element.6) | copy-start | bytes 1572868
  13.6 9.5 %collective-permute-start = (bf16[128,2048]{1,0:T(8,128)(2,1)S(1)}, bf16[128,2048]{1,0:T(8,128)(2,1)S(1)}, u32[]{:S(2)}, u32[]{:S(2)}) collective-permute-start(bf16[128,2048]{1,0:T(8,128)(2,1)S(1)} %get-tuple-element.6), channel_id=1, source_target_pairs={{0,7},{1,0},{2,1},{3,2},{4,3},{5,4},{6,5},{7,6},{8,15},{9,8},{10,9... | collective-permute-start | bytes 1572872 | tf_op jit(solution)/shard_map/ppermute | solution.py:16
  23.0 26.6 %copy-start.2 = (bf16[128,2048]{1,0:T(8,128)(2,1)}, bf16[128,2048]{1,0:T(8,128)(2,1)S(1)}, u32[]{:S(2)}) copy-start(bf16[128,2048]{1,0:T(8,128)(2,1)S(1)} %collective-permute-done) | copy-start | bytes 1572868
  23.1 25.0 %collective-permute-start.1 = (bf16[256,2048]{1,0:T(8,128)(2,1)S(1)}, bf16[256,2048]{1,0:T(8,128)(2,1)S(1)}, u32[]{:S(2)}, u32[]{:S(2)}) collective-permute-start(bf16[256,2048]{1,0:T(8,128)(2,1)S(1)} %pad_maximum_fusion.1), channel_id=1, source_target_pairs={{0,6},{1,7},{2,0},{3,1},{4,2},{5,3},{6,4},{7,5},{8,14},{9,15},{10,... | collective-permute-start | bytes 3145736 | tf_op jit(solution)/shard_map/ppermute | solution.py:16
  49.6 48.3 %collective-permute-start.2 = (bf16[512,2048]{1,0:T(8,128)(2,1)}, bf16[512,2048]{1,0:T(8,128)(2,1)S(1)}, u32[]{:S(2)}, u32[]{:S(2)}) collective-permute-start(bf16[512,2048]{1,0:T(8,128)(2,1)} %pad_maximum_fusion), channel_id=1, source_target_pairs={{0,4},{1,5},{2,6},{3,7},{4,0},{5,1},{6,2},{7,3},{8,12},{9,13},{10,... | collective-permute-start | bytes 6291464 | tf_op jit(solution)/shard_map/ppermute | solution.py:16
  51.9 47.4 %copy-start.1 = (bf16[128,2048]{1,0:T(8,128)(2,1)S(1)}, bf16[128,2048]{1,0:T(8,128)(2,1)}, u32[]{:S(2)}) copy-start(bf16[128,2048]{1,0:T(8,128)(2,1)} %copy-done) | copy-start | bytes 1572868
  51.9 48.3 %copy-start.3 = (bf16[128,2048]{1,0:T(8,128)(2,1)S(1)}, bf16[128,2048]{1,0:T(8,128)(2,1)}, u32[]{:S(2)}) copy-start(bf16[128,2048]{1,0:T(8,128)(2,1)} %copy-done.2) | copy-start | bytes 1572868
Sparse Core Ops, SparseCore 0:
  9.5 54.5 all-gather.2
  66.2 55.3 all-gather.4
  136.7 52.4 reduce-scatter.1
